TPU v7x, 32 devices: a whole 2x2x4 slice. The times are simulated.
32 devices in a mesh: kv: 4 (over y, x), tp: 8 (over z, core).
Axes of the slice: x: 2, y: 2, z: 4, core: 2. Of those that a mesh axis runs over, the one named last changes fastest.
Arguments:
- tokens: bfloat16 [16, 4096], P(None, ('kv', 'tp')), may hold values from -9 to 9
- lengths: int32 [16], replicated, may hold values from 1 to 4096, 16384 in all
- gain_attn: float32 [4096], P('kv'), may hold values from 0.1 to 1.9
- w_query_nope: bfloat16 [4096, 4096], P('kv', 'tp'), may hold values from -0.09375 to 0.09375
- w_query_rope: bfloat16 [4096, 2048], P('kv', 'tp'), may hold values from -0.09375 to 0.09375
- w_latent: bfloat16 [4096, 512], P('kv'), may hold values from -0.09375 to 0.09375
- w_rope_key: bfloat16 [4096, 64], P('kv'), may hold values from -0.09375 to 0.09375
- gain_latent: float32 [512], replicated, may hold values from 0.1 to 1.9
- w_key_up: bfloat16 [512, 4096], P(None, 'tp'), may hold values from -0.75 to 0.75
- w_value_up: bfloat16 [512, 4096], P(None, 'tp'), may hold values from -0.25 to 0.25
- w_out: bfloat16 [4096, 4096], P('tp', 'kv'), may hold values from -0.25 to 0.25
- gain_mlp: float32 [4096], P('kv'), may hold values from 0.1 to 1.9
- w_up: bfloat16 [4096, 16384], P('kv', 'tp'), may hold values from -0.09375 to 0.09375
- w_down: bfloat16 [16384, 4096], P('tp', 'kv'), may hold values from -0.046875 to 0.046875
- cache_latent: bfloat16 [16, 4096, 512], P('tp', 'kv'), may hold values from -6 to 6
- cache_rope: bfloat16 [16, 4096, 64], P('tp', 'kv'), may hold values from -900 to 900
Outputs:
- mixed: bfloat16 [16, 4096], P(None, ('kv', 'tp'))
Inputs may be any that keep to these rules, and one draw needn't show every extreme that they name: `lengths`: one sequence has exactly 4096 live positions.
All inputs are finite; a program needn't handle non-finite values.
Results may differ from a plain program's by a relative error of at most 0.035.
The roundings to bfloat16 on the way count: a program that leaves them out, or rounds other values in their place, can miss the bound.
Values may be sent and summed in bfloat16 or wider, within the bound.
A program may use at most 64 MiB of HBM per device.

v0:
```python
import jax
import jax.numpy as jnp
from jax import lax
from jax.sharding import PartitionSpec as P

D = 4096
NOPE = 128
ROPE = 64
VD = 128
RANK = 512


EPS = 1e-06


def merged_2(value, axis, combine):
    everything = jax.tree.map(
        lambda part, kind: lax.all_gather(part.astype(kind), axis),
        value,
        (jnp.bfloat16, jnp.bfloat16, jnp.bfloat16),
    )

    def take(k):
        return jax.tree.map(lambda part, own: part[k].astype(own.dtype), everything, value)

    return lax.fori_loop(
        1, lax.axis_size(axis), lambda k, so_far: combine(so_far, take(k)), take(0)
    )


def rotate(values, positions):
    half_dim = values.shape[-1] // 2
    inv_freq = 10000.0 ** (-jnp.arange(half_dim, dtype=jnp.float32) / half_dim)
    angles = positions.astype(jnp.float32)[..., None] * inv_freq
    cos_part = jnp.cos(angles)
    sin_part = jnp.sin(angles)
    lower = values[..., :half_dim]
    upper = values[..., half_dim:]
    return jnp.concatenate(
        [lower * cos_part - upper * sin_part, upper * cos_part + lower * sin_part], axis=-1
    )


def combine(earlier, later):
    max_one, sum_one, out_one = earlier
    max_two, sum_two, out_two = later
    new_max = jnp.maximum(max_one, max_two)
    weight_one = sum_one * jnp.exp(max_one - new_max)
    weight_two = sum_two * jnp.exp(max_two - new_max)
    merged = weight_one + weight_two
    safe_sum = jnp.where(merged > 0, merged, 1.0)
    result = (
        weight_one[..., None] * out_one.astype(jnp.float32)
        + weight_two[..., None] * out_two.astype(jnp.float32)
    ) / safe_sum[..., None]
    return (new_max, merged, result.astype(jnp.bfloat16))


def per_device(
    tokens,
    lengths,
    gain_attn,
    w_query_nope,
    w_query_rope,
    w_latent,
    w_rope_key,
    gain_latent,
    w_key_up,
    w_value_up,
    w_out,
    gain_mlp,
    w_up,
    w_down,
    cache_latent,
    cache_rope,
):
    kv_index = lax.axis_index("kv")
    tp_index = lax.axis_index("tp")
    seq_dev = cache_latent.shape[0]
    cache_dev = cache_latent.shape[1]
    heads_dev = w_key_up.shape[1] // NOPE
    block_cols = lax.all_gather(tokens, "tp", axis=1, tiled=True)
    batch_rows = block_cols.shape[0]
    widened = block_cols.astype(jnp.float32)
    square_piece = jnp.sum(widened * widened, axis=1)
    scaled = (widened * gain_attn).astype(jnp.bfloat16)
    part_nope = jnp.dot(scaled, w_query_nope, preferred_element_type=jnp.float32)
    part_rope = jnp.dot(scaled, w_query_rope, preferred_element_type=jnp.float32)
    own_rows = lax.dynamic_slice_in_dim(scaled, tp_index * seq_dev, seq_dev, 0)
    part_latent = jnp.dot(own_rows, w_latent, preferred_element_type=jnp.float32)
    part_key = jnp.dot(own_rows, w_rope_key, preferred_element_type=jnp.float32)
    square_sum, nope_sum, rope_sum, latent_sum, key_sum = lax.psum(
        (square_piece, part_nope, part_rope, part_latent, part_key), "kv"
    )
    inv_rms = lax.rsqrt(square_sum / D + EPS)
    q_nope = (nope_sum * inv_rms[:, None]).astype(jnp.bfloat16).reshape(batch_rows, heads_dev, NOPE)
    rope_raw = (rope_sum * inv_rms[:, None]).reshape(batch_rows, heads_dev, ROPE)
    q_rope = rotate(rope_raw, lengths[:, None]).astype(jnp.bfloat16)
    key_up = w_key_up.reshape(RANK, heads_dev, NOPE)
    q_latent = jnp.einsum(
        "bhn,rhn->bhr", q_nope, key_up, preferred_element_type=jnp.float32
    ).astype(jnp.bfloat16)
    latent_query, rope_query = (
        lax.all_to_all(q_latent, "tp", split_axis=0, concat_axis=1, tiled=True),
        lax.all_to_all(q_rope, "tp", split_axis=0, concat_axis=1, tiled=True),
    )
    own_inv = lax.dynamic_slice_in_dim(inv_rms, tp_index * seq_dev, seq_dev, 0)
    own_len = lax.dynamic_slice_in_dim(lengths, tp_index * seq_dev, seq_dev, 0)
    raw_latent = latent_sum * own_inv[:, None]
    latent_new = (
        raw_latent
        * lax.rsqrt(jnp.mean(raw_latent * raw_latent, axis=1, keepdims=True) + EPS)
        * gain_latent
    ).astype(jnp.bfloat16)
    key_new = rotate(key_sum * own_inv[:, None], own_len).astype(jnp.bfloat16)
    score_scale = (NOPE + ROPE) ** (-0.5)
    positions = kv_index * cache_dev + jnp.arange(cache_dev, dtype=jnp.int32)
    rotated = rotate(cache_rope.astype(jnp.float32), positions).astype(jnp.bfloat16)
    scores = (
        jnp.einsum("shr,spr->shp", latent_query, cache_latent, preferred_element_type=jnp.float32)
        + jnp.einsum("shk,spk->shp", rope_query, rotated, preferred_element_type=jnp.float32)
    ) * score_scale
    live_mask = positions[None, None, :] < own_len[:, None, None]
    block_max = jnp.max(jnp.where(live_mask, scores, -1e30), axis=2)
    exponent = jnp.where(live_mask, jnp.exp(scores - block_max[..., None]), 0.0)
    block_sum = jnp.sum(exponent, axis=2)
    weighted = jnp.einsum(
        "shp,spr->shr",
        exponent.astype(jnp.bfloat16),
        cache_latent,
        preferred_element_type=jnp.float32,
    )
    block_out = (weighted / jnp.where(block_sum > 0, block_sum, 1.0)[..., None]).astype(
        jnp.bfloat16
    )
    block_max, block_sum, block_out = merged_2((block_max, block_sum, block_out), "kv", combine)
    own_score = (
        jnp.einsum("shr,sr->sh", latent_query, latent_new, preferred_element_type=jnp.float32)
        + jnp.einsum("shk,sk->sh", rope_query, key_new, preferred_element_type=jnp.float32)
    ) * score_scale
    new_max = jnp.maximum(block_max, own_score)
    carried = block_sum * jnp.exp(block_max - new_max)
    own_weight = jnp.exp(own_score - new_max)
    o_latent = (
        (
            carried[..., None] * block_out.astype(jnp.float32)
            + own_weight[..., None] * latent_new.astype(jnp.float32)[:, None, :]
        )
        / (carried + own_weight)[..., None]
    ).astype(jnp.bfloat16)
    head_latent = lax.all_to_all(o_latent, "tp", split_axis=1, concat_axis=0, tiled=True)
    value_up = w_value_up.reshape(RANK, heads_dev, VD)
    head_out = (
        jnp.einsum("bhr,rhv->bhv", head_latent, value_up, preferred_element_type=jnp.float32)
        .astype(jnp.bfloat16)
        .reshape(batch_rows, heads_dev * VD)
    )
    attn_part = jnp.dot(head_out, w_out, preferred_element_type=jnp.float32)
    attn_sum = lax.psum(attn_part, "tp")
    resid = (widened + attn_sum).astype(jnp.bfloat16)
    resid_wide = resid.astype(jnp.float32)
    square_two = jnp.sum(resid_wide * resid_wide, axis=1)
    scaled2 = (resid_wide * gain_mlp).astype(jnp.bfloat16)
    up_part = jnp.dot(scaled2, w_up, preferred_element_type=jnp.float32)
    spread_squares = jnp.broadcast_to(square_two[:, None], (batch_rows, lax.axis_size("kv")))
    up_share, square_cols = (
        lax.psum_scatter(up_part, "kv", scatter_dimension=1, tiled=True),
        lax.psum_scatter(spread_squares, "kv", scatter_dimension=1, tiled=True),
    )
    square_all = square_cols[:, 0]
    active_share = jnp.square(jnp.maximum(up_share, 0.0)).astype(jnp.bfloat16)
    activated = lax.all_gather(active_share, "kv", axis=1, tiled=True)
    inv_rms2 = lax.rsqrt(square_all / D + EPS)
    down_part = jnp.dot(activated, w_down, preferred_element_type=jnp.float32)
    down_sum = lax.psum_scatter(down_part, "tp", scatter_dimension=1, tiled=True)
    out_cols = down_sum.shape[1]
    resid_cols = lax.dynamic_slice_in_dim(resid_wide, tp_index * out_cols, out_cols, 1)
    return (resid_cols + (inv_rms2 * inv_rms2)[:, None] * down_sum).astype(jnp.bfloat16)


def solution(mesh):
    in_specs = (
        P(None, ("kv", "tp")),
        P(),
        P("kv"),
        P("kv", "tp"),
        P("kv", "tp"),
        P("kv", None),
        P("kv", None),
        P(),
        P(None, "tp"),
        P(None, "tp"),
        P("tp", "kv"),
        P("kv"),
        P("kv", "tp"),
        P("tp", "kv"),
        P("tp", "kv", None),
        P("tp", "kv", None),
    )
    out_specs = P(None, ("kv", "tp"))
    return jax.shard_map(
        per_device, mesh=mesh, in_specs=in_specs, out_specs=out_specs, check_vma=False
    )
```

profile of v0, /device:TPU:0, one launch (start us, length us, event | category | flops | bytes accessed | tf_op | source)
XLA Modules:
  0.0 232.3 jit_solution(9144840730613302866)
XLA Ops:
  7.4 14.6 %all_gather.20 = bf16[16,1024]{1,0:T(8,128)(2,1)S(1)} all-gather(bf16[16,128]{1,0:T(8,128)(2,1)} %param.18), channel_id=1, replica_groups=mesh['kv'=4,'tp'=8] {'tp'}, dimensions={1}, use_global_device_ids=true | all-gather | bytes 36864 | tf_op jit(solution)/shard_map/all_gather | solution.py:82
  22.8 1.0 fusion.39
  23.8 1.5 fusion.41
  25.3 1.2 fusion.73
  26.5 1.5 fusion.71
  28.0 17.0 %all-reduce.1 = (f32[16,512]{1,0:T(8,128)S(1)}, f32[16]{0:T(128)S(1)}, f32[16,256]{1,0:T(8,128)S(1)}, f32[2,512]{1,0:T(2,128)S(1)}, f32[2,64]{1,0:T(2,128)S(1)}) all-reduce(f32[16,512]{1,0:T(8,128)S(1)} %fusion.71, f32[16]{0:T(128)S(1)} %get-tuple-element.223, f32[16,256]{1,0:T(8,128)S(1)} %fusion.73, ...), channel_id=1, replica_groups=mesh['kv'=4,'tp'=8] {'kv'}, use_global_device_ids=true, to_apply=%region_0.0 | all-reduce | flops 13456 | bytes 107648 | tf_op jit(solution)/shard_map/psum | solution.py:92
  46.2 3.4 %all-to-all-start.1 = ((bf16[8,2,256]{2,1,0:T(2,128)(2,1)}), bf16[8,2,256]{2,1,0:T(2,128)(2,1)S(1)}, u32[]{:S(2)}, u32[]{:S(2)}) async-start(bf16[8,2,256]{2,1,0:T(2,128)(2,1)} %reshape.265), calls=%async_computation.1 | async-start | bytes 16384 | tf_op jit(solution)/shard_map/all_to_all | solution.py:105
  51.2 1.0 convert_element_type.177
  53.6 1.6 all-to-all-done.1
  55.2 3.5 %all-to-all-start = ((bf16[16,4,512]{2,1,0:T(4,128)(2,1)}), bf16[16,4,512]{2,1,0:T(4,128)(2,1)S(1)}, u32[]{:S(2)}, u32[]{:S(2)}) async-start(bf16[16,4,512]{2,1,0:T(4,128)(2,1)} %copy.32), calls=%async_computation | async-start | bytes 131072 | tf_op jit(solution)/shard_map/all_to_all | solution.py:104
  59.0 5.7 %all-to-all-done = bf16[16,4,512]{2,1,0:T(4,128)(2,1)S(1)} async-done(((bf16[16,4,512]{2,1,0:T(4,128)(2,1)}), bf16[16,4,512]{2,1,0:T(4,128)(2,1)S(1)}, u32[]{:S(2)}, u32[]{:S(2)}) %all-to-all-start) | async-done | bytes 65568 | tf_op jit(solution)/shard_map/all_to_all | solution.py:104
  66.5 7.1 %all-gather.3 = bf16[4,2,32]{2,1,0:T(2,128)(2,1)S(1)} all-gather(bf16[1,2,32]{2,1,0:T(2,128)(2,1)S(1)} %convert_bitcast_fusion.1), channel_id=2, replica_groups=mesh['kv'=4,'tp'=8] {'kv'}, dimensions={0}, use_global_device_ids=true | all-gather | bytes 640 | tf_op jit(solution)/shard_map/all_gather | solution.py:18
  73.7 7.8 %all-gather.4 = bf16[4,2,32]{2,1,0:T(2,128)(2,1)S(1)} all-gather(bf16[1,2,32]{2,1,0:T(2,128)(2,1)S(1)} %get-tuple-element.230), channel_id=3, replica_groups=mesh['kv'=4,'tp'=8] {'kv'}, dimensions={0}, use_global_device_ids=true | all-gather | bytes 640 | tf_op jit(solution)/shard_map/all_gather | solution.py:18
  81.4 8.1 %all-gather.2 = bf16[8,32,512]{2,1,0:T(8,128)(2,1)S(1)} all-gather(bf16[2,32,512]{2,1,0:T(8,128)(2,1)S(1)} %fusion.8), channel_id=4, replica_groups=mesh['kv'=4,'tp'=8] {'kv'}, dimensions={0}, use_global_device_ids=true | all-gather | bytes 327680 | tf_op jit(solution)/shard_map/all_gather | solution.py:18
  90.5 8.3 %all_to_all.54 = bf16[2,32,512]{2,0,1:T(2,128)(2,1)S(1)} all-to-all(bf16[2,32,512]{2,0,1:T(2,128)(2,1)S(1)} %fusion.21), channel_id=1, replica_groups=mesh['kv'=4,'tp'=8] {'tp'}, dimensions={1} | all-to-all | bytes 131072 | tf_op jit(solution)/shard_map/all_to_all | solution.py:151
  98.9 1.2 fusion.10
  101.1 52.4 %all-reduce.4.cloned.1.call-done = f32[16,1024]{1,0:T(8,128)} async-done(((f32[16,1024]{1,0:T(8,128)}), f32[16,1024]{1,0:T(8,128)}) %all-reduce.4.cloned.1.call-update) | async-done | bytes 65552 | tf_op jit(solution)/shard_map/psum | solution.py:159
  154.5 3.5 %fusion.28 = f32[16,2048]{1,0:T(8,128)} fusion(bf16[1024,2048]{1,0:T(8,128)(2,1)} %param.30, f32[16,1024]{1,0:T(8,128)S(1)} %get-tuple-element.211, f32[1024]{0:T(1024)S(1)} %copy-done.3), kind=kOutput, calls=%fused_computation.52 | convolution fusion | flops 67141632 | bytes 4395008 | tf_op jit(solution)/shard_map/dot_general | solution.py:164
  158.0 23.3 %reduce-scatter.3.cloned.1.call-done = f32[16,512]{1,0:T(8,128)} async-done(((f32[16,2048]{1,0:T(8,128)}), f32[16,512]{1,0:T(8,128)}) %reduce-scatter.3.cloned.1.call-update) | async-done | bytes 32784 | tf_op jit(solution)/shard_map/reduce_scatter | solution.py:167
  182.1 8.2 %all_gather.25 = bf16[16,2048]{1,0:T(8,128)(2,1)S(1)} all-gather(bf16[16,512]{1,0:T(8,128)(2,1)S(1)} %multiply_convert_fusion.2), channel_id=1, replica_groups=mesh['kv'=4,'tp'=8] {'kv'}, dimensions={1}, use_global_device_ids=true | all-gather | bytes 81920 | tf_op jit(solution)/shard_map/all_gather | solution.py:172
  190.3 3.5 %fusion.74 = f32[16,1024]{1,0:T(8,128)} fusion(bf16[16,2048]{1,0:T(8,128)(2,1)S(1)} %all_gather.25, bf16[2048,1024]{1,0:T(8,128)(2,1)} %param.31), kind=kOutput, calls=%fused_computation.124 | convolution fusion | flops 67108864 | bytes 4325376 | tf_op jit(solution)/shard_map/dot_general | solution.py:174
  194.4 8.9 %all-reduce = f32[16,4]{0,1:T(4,128)S(1)} all-reduce(f32[16,4]{0,1:T(4,128)S(1)} %broadcast_in_dim.47), channel_id=5, replica_groups=mesh['kv'=4,'tp'=8] {'kv'}, use_global_device_ids=true, to_apply=%region_13.14.clone | all-reduce | flops 64 | bytes 512
  204.0 20.4 %reduce-scatter.5.cloned.1.call-done = f32[16,128]{1,0:T(8,128)} async-done(((f32[16,1024]{1,0:T(8,128)}), f32[16,128]{1,0:T(8,128)}) %reduce-scatter.5.cloned.1.call-update) | async-done | bytes 8208 | tf_op jit(solution)/shard_map/reduce_scatter | solution.py:175
  224.4 1.4 add_convert_fusion.2
  (77 shorter events, 13.3 us)
Async XLA Ops:
  6.5 58.3 %copy-start = (bf16[2,1024,512]{2,1,0:T(8,128)(2,1)S(1)}, bf16[2,1024,512]{2,1,0:T(8,128)(2,1)}, u32[]{:S(2)}) copy-start(bf16[2,1024,512]{2,1,0:T(8,128)(2,1)} %param.32) | copy-start | bytes 6291460
  6.5 45.9 %copy-start.4 = (f32[512]{0:T(512)S(1)}, f32[512]{0:T(512)}, u32[]{:S(2)}) copy-start(f32[512]{0:T(512)} %param.25) | copy-start | bytes 6148
  6.5 46.0 %copy-start.2 = (bf16[512,512]{1,0:T(8,128)(2,1)S(1)}, bf16[512,512]{1,0:T(8,128)(2,1)}, u32[]{:S(2)}) copy-start(bf16[512,512]{1,0:T(8,128)(2,1)} %param.26) | copy-start | bytes 1572868
  46.2 9.0 %all-to-all-start.1 = ((bf16[8,2,256]{2,1,0:T(2,128)(2,1)}), bf16[8,2,256]{2,1,0:T(2,128)(2,1)S(1)}, u32[]{:S(2)}, u32[]{:S(2)}) async-start(bf16[8,2,256]{2,1,0:T(2,128)(2,1)} %reshape.265), calls=%async_computation.1 | async-start | bytes 16384 | tf_op jit(solution)/shard_map/all_to_all | solution.py:105
  55.2 9.4 %all-to-all-start = ((bf16[16,4,512]{2,1,0:T(4,128)(2,1)}), bf16[16,4,512]{2,1,0:T(4,128)(2,1)S(1)}, u32[]{:S(2)}, u32[]{:S(2)}) async-start(bf16[16,4,512]{2,1,0:T(4,128)(2,1)} %copy.32), calls=%async_computation | async-start | bytes 131072 | tf_op jit(solution)/shard_map/all_to_all | solution.py:104
  58.7 94.8 %all-reduce.4.cloned.1.call-start = ((), (), s32[]{:S(2)}) async-start(), calls=%async_computation.5 | async-start | bytes 131072 | tf_op jit(solution)/shard_map/psum | solution.py:159
  64.8 35.3 %copy-start.1 = (bf16[512,1024]{1,0:T(8,128)(2,1)S(1)}, bf16[512,1024]{1,0:T(8,128)(2,1)}, u32[]{:S(2)}) copy-start(bf16[512,1024]{1,0:T(8,128)(2,1)} %param.28) | copy-start | bytes 3145732
  65.5 88.9 %copy-start.3 = (f32[1024]{0:T(1024)S(1)}, f32[1024]{0:T(1024)}, u32[]{:S(2)}) copy-start(f32[1024]{0:T(1024)} %param.29) | copy-start | bytes 12292
  101.1 80.3 %reduce-scatter.3.cloned.1.call-start = ((), (), s32[]{:S(2)}) async-start(), calls=%async_computation.6 | async-start | bytes 163840 | tf_op jit(solution)/shard_map/reduce_scatter | solution.py:167
  154.5 39.3 %copy-start.5 = (u32[32]{0:T(128)S(1)}, u32[32]{0:T(128)}, u32[]{:S(2)}) copy-start(u32[32]{0:T(128)} %constant.104) | copy-start | bytes 388
  158.0 66.4 %reduce-scatter.5.cloned.1.call-start = ((), (), s32[]{:S(2)}) async-start(), calls=%async_computation.7 | async-start | bytes 73728 | tf_op jit(solution)/shard_map/reduce_scatter | solution.py:175
Sparse Core Ops, SparseCore 0:
  101.2 52.2 all-reduce.3
  158.1 23.2 reduce-scatter.2
  193.9 30.4 reduce-scatter.4
where the time goes:
time: 233 us; the launch traced here: 232 us
  waiting for transfers between devices  103 us (44%)
  blocking collectives  80 us (34%)
  matrix products  16.3 us (7%)
  between operations  13.3 us (6%)
  other arithmetic  9.51 us (4%)
  starting transfers between devices  7.03 us (3%)
  local copies, waits for them, and re-layouts  2.62 us (1%)
    psum x1, waiting for transfers between devices, per_device(): attn_sum = lax.psum(attn_part, 'tp')  52.4 us
    reduce_scatter x1, waiting for transfers between devices, per_device(): lax.psum_scatter(up_part, 'kv', scatter_dimension=1, tiled=True)  23.3 us
    all_gather x3, blocking collectives, merged_2(): lax.all_gather(part.astype(kind), axis)  23 us
    reduce_scatter x1, waiting for transfers between devices, per_device(): lax.psum_scatter(down_part, 'tp', scatter_dimension=1, tiled=True)  20.4 us
    psum x1, blocking collectives, per_device(): lax.psum((square_piece, part_nope, part_rope, part_latent, part_key), 'kv')  17 us
    all_gather x1, blocking collectives, per_device(): block_cols = lax.all_gather(tokens, 'tp', axis=1, tiled=True)  14.6 us
    unnamed x1, blocking collectives  8.89 us
    all_to_all x1, blocking collectives, per_device(): lax.all_to_all(o_latent, 'tp', split_axis=1, concat_axis=0, tiled=True)  8.3 us
  transfers between devices with their start and end apart: 5, of which 5 were waited for; matrix products, arithmetic and copies ran while one was open for 2% of the time, Pallas kernels for 0%

commit v1 on v0

--- a/solution.py
+++ b/solution.py
@@ -1,6 +1,11 @@
+import functools
+
 import jax
 import jax.numpy as jnp
+import numpy as np
 from jax import lax
+from jax.experimental import pallas as pl
+from jax.experimental.pallas import tpu as pltpu
 from jax.sharding import PartitionSpec as P
 
 D = 4096
@@ -178,7 +183,521 @@
     return (resid_cols + (inv_rms2 * inv_rms2)[:, None] * down_sum).astype(jnp.bfloat16)
 
 
+MESH = pl.DeviceIdType.MESH
+BF16 = jnp.bfloat16
+F32 = jnp.float32
+FINE = 32
+
+
+def dot(a, b):
+    return jnp.dot(a, b, preferred_element_type=F32)
+
+
+def dot_nt(a, b):
+    return lax.dot_general(a, b, (((1,), (1,)), ((), ())), preferred_element_type=F32)
+
+
+def iota(shape, axis):
+    return lax.broadcasted_iota(jnp.int32, shape, axis)
+
+
+def layer_kernel(
+    n_kv,
+    n_tp,
+    len_ref,
+    tok_ref,
+    gain_attn,
+    gain_latent,
+    gain_mlp,
+    coarse_ref,
+    fine_ref,
+    freq_ref,
+    h_qn,
+    h_qr,
+    h_lat,
+    h_key,
+    h_kup,
+    h_vup,
+    h_out,
+    h_up,
+    h_down,
+    h_cl,
+    h_cr,
+    out_ref,
+    w_qn,
+    w_qr,
+    w_lat,
+    w_key,
+    w_kup,
+    w_vup,
+    w_out,
+    w_up,
+    w_down,
+    c_lat,
+    c_rope,
+    rot,
+    tok_all,
+    qp_own,
+    qp_in,
+    lat_own,
+    lat_in,
+    sq_own,
+    sq_in,
+    q_own,
+    q_in,
+    bo_own,
+    bo_in,
+    st_own,
+    st_in,
+    o_own,
+    o_in,
+    ap_own,
+    ap_in,
+    res_own,
+    res_all,
+    up_own,
+    up_in,
+    sq2_own,
+    sq2_in,
+    act_own,
+    act_all,
+    dn_own,
+    dn_in,
+    load_sem,
+    send_sem,
+    recv_sem,
+):
+    kv = lax.axis_index("kv")
+    tp = lax.axis_index("tp")
+    size = {"kv": n_kv, "tp": n_tp}
+    here = {"kv": kv, "tp": tp}
+    batch, col = tok_ref.shape
+    seqs, cache_dev, rank = c_lat.shape
+    heads = w_kup.shape[1] // NOPE
+    rows = batch * heads
+    group = seqs * heads
+    n_nope = heads * NOPE
+    n_rope = heads * ROPE
+
+    loads = {}
+    order = (
+        ("qn", h_qn, w_qn),
+        ("qr", h_qr, w_qr),
+        ("lat", h_lat, w_lat),
+        ("key", h_key, w_key),
+        ("cr", h_cr, c_rope),
+        ("kup", h_kup, w_kup),
+        ("cl", h_cl, c_lat),
+        ("vup", h_vup, w_vup),
+        ("out", h_out, w_out),
+        ("up", h_up, w_up),
+        ("down", h_down, w_down),
+    )
+    for i, (name, hbm, vmem) in enumerate(order):
+        loads[name] = pltpu.make_async_copy(hbm, vmem, load_sem.at[i])
+        loads[name].start()
+
+    barrier = pltpu.get_barrier_semaphore()
+    for axis in ("kv", "tp"):
+        for d in range(1, size[axis]):
+            pl.semaphore_signal(
+                barrier,
+                inc=1,
+                device_id={axis: lax.rem(here[axis] + d, size[axis])},
+                device_id_type=MESH,
+            )
+
+    started = []
+
+    def send(axis, d, source, target):
+        i = len(started)
+        copy = pltpu.make_async_remote_copy(
+            src_ref=source,
+            dst_ref=target,
+            send_sem=send_sem.at[i],
+            recv_sem=recv_sem.at[i],
+            device_id={axis: lax.rem(here[axis] + d, size[axis])},
+            device_id_type=MESH,
+        )
+        copy.start()
+        started.append(copy)
+        return copy
+
+    def peer(axis, d):
+        return lax.rem(here[axis] + d, size[axis])
+
+    def arrive(copies):
+        for copy in copies:
+            copy.wait_recv()
+
+    lane_r = iota((batch, n_rope), 1)
+    row_b = iota((batch, n_rope), 0)
+    len_b = jnp.zeros((batch, n_rope), jnp.int32)
+    for b in range(batch):
+        len_b = jnp.where(row_b == b, len_ref[b], len_b)
+    angle = len_b.astype(F32) * freq_ref[0:1, :n_rope]
+    q_cos = jnp.cos(angle)
+    q_sin = jnp.sin(angle)
+    lane_k = iota((group, 128), 1)
+    row_k = iota((group, 128), 0) // heads
+    len_k = jnp.zeros((group, 128), jnp.int32)
+    for s in range(seqs):
+        len_k = jnp.where(row_k == s, len_ref[tp * seqs + s], len_k)
+    angle_k = len_k.astype(F32) * freq_ref[0:1, :128]
+    k_cos = jnp.cos(angle_k)
+    k_sin = jnp.sin(angle_k)
+
+    spread = (iota((rows, batch), 0) // heads == iota((rows, batch), 1)).astype(F32).astype(BF16)
+    gather = (iota((batch, rows), 1) // heads == iota((batch, rows), 0)).astype(F32).astype(BF16)
+    pick = (iota((group, batch), 0) // heads + tp * seqs == iota((group, batch), 1))
+    pick = pick.astype(F32).astype(BF16)
+
+    pl.semaphore_wait(barrier, n_kv + n_tp - 2)
+
+    tok_copies = [send("tp", d, tok_ref, tok_all.at[tp]) for d in range(1, n_tp)]
+    tok_all[tp] = tok_ref[...]
+
+    loads["cr"].wait()
+    half = ROPE // 2
+    s_row = iota((ROPE, ROPE), 0)
+    s_col = iota((ROPE, ROPE), 1)
+    swap = jnp.where(s_row == s_col + half, -1.0, 0.0) + jnp.where(s_row + half == s_col, 1.0, 0.0)
+    swap = swap.astype(BF16)
+    n_coarse = cache_dev // FINE
+    first = pl.multiple_of(kv * n_coarse, 8)
+    cos_a = coarse_ref[0, pl.ds(first, n_coarse), :]
+    sin_a = coarse_ref[1, pl.ds(first, n_coarse), :]
+    cos_b = fine_ref[0]
+    sin_b = fine_ref[1]
+    for i in range(n_coarse):
+        part = pl.ds(i * FINE, FINE)
+        ca, sa = cos_a[i : i + 1], sin_a[i : i + 1]
+        cos_p = ca * cos_b - sa * sin_b
+        sin_p = sa * cos_b + ca * sin_b
+        for s in range(seqs):
+            keys = c_rope[s, part, :]
+            turned = keys.astype(F32) * cos_p + dot(keys, swap) * sin_p
+            rot[s, part, :] = turned.astype(BF16)
+
+    arrive(tok_copies)
+    toks = jnp.concatenate([tok_all[i] for i in range(n_tp)], axis=1)
+    wide = toks.astype(F32)
+    scaled = (wide * gain_attn[...]).astype(BF16)
+    loads["qn"].wait()
+    qp_own[:, :n_nope] = dot(scaled, w_qn[...]).astype(BF16)
+    loads["qr"].wait()
+    qp_own[:, n_nope:] = dot(scaled, w_qr[...]).astype(BF16)
+    sq_own[...] = jnp.broadcast_to(jnp.sum(wide * wide, axis=1, keepdims=True), sq_own.shape)
+    qp_copies = [send("kv", d, qp_own, qp_in.at[d - 1]) for d in range(1, n_kv)]
+    sq_copies = [send("kv", d, sq_own, sq_in.at[d - 1]) for d in range(1, n_kv)]
+    own_tok = dot(pick, toks)
+    own_scaled = (own_tok * gain_attn[...]).astype(BF16)
+    loads["lat"].wait()
+    lat_own[:, :rank] = dot(own_scaled, w_lat[...])
+    loads["key"].wait()
+    lat_own[:, rank : rank + ROPE] = dot(own_scaled, w_key[...])
+    lat_own[:, rank + ROPE :] = jnp.broadcast_to(
+        jnp.sum(own_tok * own_tok, axis=1, keepdims=True), (group, ROPE)
+    )
+    lat_copies = [send("kv", d, lat_own, lat_in.at[d - 1]) for d in range(1, n_kv)]
+
+    loads["kup"].wait()
+    arrive(qp_copies)
+    arrive(sq_copies)
+    q_sum = qp_own[...].astype(F32)
+    square = sq_own[:, 0:1]
+    for d in range(n_kv - 1):
+        q_sum = q_sum + qp_in[d].astype(F32)
+        square = square + sq_in[d, :, 0:1]
+    q_sum = q_sum * lax.rsqrt(square / D + EPS)
+    q_nope = q_sum[:, :n_nope].astype(BF16)
+    raw = q_sum[:, n_nope:]
+    swapped = jnp.where(
+        lane_r % ROPE < half, -pltpu.roll(raw, n_rope - half, 1), pltpu.roll(raw, half, 1)
+    )
+    q_rope = (raw * q_cos + swapped * q_sin).astype(BF16)
+    own_cols = iota((rows, n_nope), 1) // NOPE == iota((rows, n_nope), 0) % heads
+    own_rope = iota((rows, n_rope), 1) // ROPE == iota((rows, n_rope), 0) % heads
+    q_wide = jnp.where(own_cols, dot(spread, q_nope), 0.0).astype(BF16)
+    q_lat = dot_nt(q_wide, w_kup[...])
+    r_wide = jnp.where(own_rope, dot(spread, q_rope), 0.0).astype(BF16)
+    fold = (iota((n_rope, 128), 0) % ROPE == iota((n_rope, 128), 1)).astype(F32).astype(BF16)
+    q_rot = dot(r_wide, fold)
+    q_own[:, :, :rank] = q_lat.reshape(n_tp, group, rank).astype(BF16)
+    q_own[:, :, rank:] = q_rot.reshape(n_tp, group, 128).astype(BF16)
+    q_copies = [
+        send("tp", d, q_own.at[peer("tp", d)], q_in.at[tp]) for d in range(1, n_tp)
+    ]
+    q_in[tp] = q_own[tp]
+
+    arrive(lat_copies)
+    lat_sum = lat_own[...]
+    for d in range(n_kv - 1):
+        lat_sum = lat_sum + lat_in[d]
+    own_inv = lax.rsqrt(lat_sum[:, rank + ROPE : rank + ROPE + 1] / D + EPS)
+    raw_latent = lat_sum[:, :rank] * own_inv
+    mean_sq = jnp.mean(raw_latent * raw_latent, axis=1, keepdims=True)
+    latent_new = (raw_latent * lax.rsqrt(mean_sq + EPS) * gain_latent[...]).astype(BF16).astype(F32)
+    raw_key = lat_sum[:, rank:] * own_inv
+    raw_key = jnp.where(lane_k < ROPE, raw_key, pltpu.roll(raw_key, ROPE, 1))
+    swap_key = jnp.where(
+        lane_k % ROPE < half, -pltpu.roll(raw_key, 128 - half, 1), pltpu.roll(raw_key, half, 1)
+    )
+    key_new = (raw_key * k_cos + swap_key * k_sin).astype(BF16).astype(F32)
+    key_new = jnp.where(lane_k < ROPE, key_new, 0.0)
+    latent_rows = jnp.broadcast_to(latent_new[None], (n_tp, group, rank)).reshape(rows, rank)
+    key_rows = jnp.broadcast_to(key_new[None], (n_tp, group, 128)).reshape(rows, 128)
+
+    row_seq = iota((rows, 1), 0) % group // heads
+    own_len = jnp.zeros((rows, 1), jnp.int32)
+    for s in range(seqs):
+        own_len = jnp.where(row_seq == s, len_ref[tp * seqs + s], own_len)
+    score_scale = (NOPE + ROPE) ** (-0.5)
+
+    loads["cl"].wait()
+    arrive(q_copies)
+    q_all = q_in[...].astype(F32).reshape(rows, rank + 128)
+    q_low = q_all.astype(BF16)
+    latent_query = q_low[:, :rank]
+    rope_query = q_low[:, rank : rank + ROPE]
+    scores = None
+    for s in range(seqs):
+        one = dot_nt(latent_query, c_lat[s]) + dot_nt(rope_query, rot[s])
+        scores = one if scores is None else jnp.where(row_seq == s, one, scores)
+    scores = scores * score_scale
+    live = kv * cache_dev + iota((rows, cache_dev), 1) < own_len
+    block_max = jnp.max(jnp.where(live, scores, -1e30), axis=1, keepdims=True)
+    expo = jnp.where(live, jnp.exp(scores - block_max), 0.0)
+    block_sum = jnp.sum(expo, axis=1, keepdims=True)
+    expo_low = expo.astype(BF16)
+    weighted = None
+    for s in range(seqs):
+        one = dot(expo_low, c_lat[s])
+        weighted = one if weighted is None else jnp.where(row_seq == s, one, weighted)
+    bo_own[...] = (weighted / jnp.where(block_sum > 0, block_sum, 1.0)).astype(BF16)
+    diag = iota((rows, 128), 0) == iota((rows, 128), 1)
+    max_row = jnp.sum(jnp.where(diag, block_max, 0.0), axis=0, keepdims=True)
+    sum_row = jnp.sum(jnp.where(diag, block_sum, 0.0), axis=0, keepdims=True)
+    st_own[...] = jnp.where(iota((8, 128), 0) == 0, max_row, sum_row)
+    bo_copies = [send("kv", d, bo_own, bo_in.at[d - 1]) for d in range(1, n_kv)]
+    st_copies = [send("kv", d, st_own, st_in.at[d - 1]) for d in range(1, n_kv)]
+
+    self_score = (
+        jnp.sum(q_all[:, :rank] * latent_rows, axis=1, keepdims=True)
+        + jnp.sum(q_all[:, rank:] * key_rows, axis=1, keepdims=True)
+    ) * score_scale
+    arrive(st_copies)
+    maxes, sums = [block_max], [block_sum]
+    for d in range(n_kv - 1):
+        maxes.append(jnp.sum(jnp.where(diag, st_in[d, 0:1, :], 0.0), axis=1, keepdims=True))
+        sums.append(jnp.sum(jnp.where(diag, st_in[d, 1:2, :], 0.0), axis=1, keepdims=True))
+    top = self_score
+    for one in maxes:
+        top = jnp.maximum(top, one)
+    weights = [total * jnp.exp(one - top) for one, total in zip(maxes, sums)]
+    self_weight = jnp.exp(self_score - top)
+    whole = self_weight
+    for one in weights:
+        whole = whole + one
+    blend = self_weight * latent_rows + weights[0] * bo_own[...].astype(F32)
+    for d in range(n_kv - 1):
+        bo_copies[d].wait_recv()
+        blend = blend + weights[d + 1] * bo_in[d].astype(F32)
+    o_own[...] = (blend / whole).reshape(n_tp, group, rank).astype(BF16)
+    o_copies = [
+        send("tp", d, o_own.at[peer("tp", d)], o_in.at[tp]) for d in range(1, n_tp)
+    ]
+    o_in[tp] = o_own[tp]
+    loads["vup"].wait()
+    loads["out"].wait()
+    arrive(o_copies)
+    o_low = o_in[...].astype(F32).reshape(rows, rank).astype(BF16)
+    v_cols = iota((rows, heads * VD), 1) // VD == iota((rows, heads * VD), 0) % heads
+    v_wide = jnp.where(v_cols, dot(o_low, w_vup[...]), 0.0).astype(BF16)
+    head_out = dot(gather, v_wide).astype(BF16)
+
+    attn = dot(head_out, w_out[...])
+    for i in range(n_tp):
+        ap_own[i] = attn[:, i * col : (i + 1) * col].astype(BF16)
+    ap_copies = [
+        send("tp", d, ap_own.at[peer("tp", d)], ap_in.at[d - 1]) for d in range(1, n_tp)
+    ]
+    resid = tok_ref[...].astype(F32) + ap_own[tp].astype(F32)
+    for d in range(n_tp - 1):
+        ap_copies[d].wait_recv()
+        resid = resid + ap_in[d].astype(F32)
+    res_own[...] = resid.astype(BF16)
+    res_copies = [send("tp", d, res_own, res_all.at[tp]) for d in range(1, n_tp)]
+    resid = res_own[...].astype(F32)
+    res_all[tp] = res_own[...]
+    loads["up"].wait()
+    arrive(res_copies)
+    wide2 = jnp.concatenate([res_all[i] for i in range(n_tp)], axis=1).astype(F32)
+    sq2_own[...] = jnp.broadcast_to(jnp.sum(wide2 * wide2, axis=1, keepdims=True), sq2_own.shape)
+    scaled2 = (wide2 * gain_mlp[...]).astype(BF16)
+    sq2_copies = [send("kv", d, sq2_own, sq2_in.at[d - 1]) for d in range(1, n_kv)]
+    share = w_up.shape[1] // n_kv
+    up_copies = []
+    for d in range(1, n_kv):
+        cols = pl.ds(pl.multiple_of(peer("kv", d) * share, 128), share)
+        up_own[d - 1] = dot(scaled2, w_up[:, cols]).astype(BF16)
+        up_copies.append(send("kv", d, up_own.at[d - 1], up_in.at[d - 1]))
+    up_sum = dot(scaled2, w_up[:, pl.ds(pl.multiple_of(kv * share, 128), share)])
+    for d in range(n_kv - 1):
+        up_copies[d].wait_recv()
+        up_sum = up_sum + up_in[d].astype(F32)
+    act_own[...] = jnp.square(jnp.maximum(up_sum, 0.0)).astype(BF16)
+    act_copies = [send("kv", d, act_own, act_all.at[d - 1]) for d in range(1, n_kv)]
+    loads["down"].wait()
+    down = dot(act_own[...], w_down[pl.ds(pl.multiple_of(kv * share, 128), share), :])
+    for d in range(1, n_kv):
+        act_copies[d - 1].wait_recv()
+        source = lax.rem(kv + n_kv - d, n_kv)
+        down = down + dot(
+            act_all[d - 1], w_down[pl.ds(pl.multiple_of(source * share, 128), share), :]
+        )
+    for i in range(n_tp):
+        dn_own[i] = down[:, i * col : (i + 1) * col].astype(BF16)
+    dn_copies = [
+        send("tp", d, dn_own.at[peer("tp", d)], dn_in.at[d - 1]) for d in range(1, n_tp)
+    ]
+    arrive(sq2_copies)
+    square2 = sq2_own[:, 0:1]
+    for d in range(n_kv - 1):
+        square2 = square2 + sq2_in[d, :, 0:1]
+    inv2 = lax.rsqrt(square2 / D + EPS)
+    total = dn_own[tp].astype(F32)
+    for d in range(n_tp - 1):
+        dn_copies[d].wait_recv()
+        total = total + dn_in[d].astype(F32)
+    out_ref[...] = (resid + (inv2 * inv2) * total).astype(BF16)
+    for copy in started:
+        copy.wait_send()
+
+
+def fused(
+    n_kv,
+    n_tp,
+    tokens,
+    lengths,
+    gain_attn,
+    w_query_nope,
+    w_query_rope,
+    w_latent,
+    w_rope_key,
+    gain_latent,
+    w_key_up,
+    w_value_up,
+    w_out,
+    gain_mlp,
+    w_up,
+    w_down,
+    cache_latent,
+    cache_rope,
+):
+    batch, col = tokens.shape
+    seqs, cache_dev, rank = cache_latent.shape
+    heads = w_key_up.shape[1] // NOPE
+    rows, group = batch * heads, seqs * heads
+    share = w_up.shape[1] // n_kv
+    half = ROPE // 2
+    freq = np.float32(10000.0) ** (-np.arange(half, dtype=np.float32) / np.float32(half))
+    freq = freq.astype(np.float64)
+    lanes = np.tile(freq, 2)[None, :]
+    coarse = np.arange(n_kv * cache_dev // FINE)[:, None] * FINE * lanes
+    fine = np.arange(FINE)[:, None] * lanes
+    coarse = jnp.asarray(np.stack([np.cos(coarse), np.sin(coarse)]), F32)
+    fine = jnp.asarray(np.stack([np.cos(fine), np.sin(fine)]), F32)
+    wide_lanes = max(heads * ROPE, 128)
+    freq_row = jnp.asarray(np.tile(np.tile(freq, wide_lanes // half)[None, :], (8, 1)), F32)
+
+    def vm(*shape, kind=BF16):
+        return pltpu.VMEM(shape, kind)
+
+    weights = (
+        w_query_nope,
+        w_query_rope,
+        w_latent,
+        w_rope_key,
+        w_key_up,
+        w_value_up,
+        w_out,
+        w_up,
+        w_down,
+        cache_latent,
+        cache_rope,
+    )
+    k, t = n_kv - 1, n_tp - 1
+    qp = heads * (NOPE + ROPE)
+    scratch = [vm(*w.shape, kind=w.dtype) for w in weights] + [
+        vm(*cache_rope.shape),
+        vm(n_tp, batch, col),
+        vm(batch, qp),
+        vm(k, batch, qp),
+        vm(group, rank + 2 * ROPE, kind=F32),
+        vm(k, group, rank + 2 * ROPE, kind=F32),
+        vm(batch, 128, kind=F32),
+        vm(k, batch, 128, kind=F32),
+        vm(n_tp, group, rank + 128),
+        vm(n_tp, group, rank + 128),
+        vm(rows, rank),
+        vm(k, rows, rank),
+        vm(8, 128, kind=F32),
+        vm(k, 8, 128, kind=F32),
+        vm(n_tp, group, rank),
+        vm(n_tp, group, rank),
+        vm(n_tp, batch, col),
+        vm(t, batch, col),
+        vm(batch, col),
+        vm(n_tp, batch, col),
+        vm(k, batch, share),
+        vm(k, batch, share),
+        vm(batch, 128, kind=F32),
+        vm(k, batch, 128, kind=F32),
+        vm(batch, share),
+        vm(k, batch, share),
+        vm(n_tp, batch, col),
+        vm(t, batch, col),
+        pltpu.SemaphoreType.DMA((len(weights),)),
+        pltpu.SemaphoreType.DMA((6 * t + 8 * k,)),
+        pltpu.SemaphoreType.DMA((6 * t + 8 * k,)),
+    ]
+    in_vmem = pl.BlockSpec(memory_space=pltpu.VMEM)
+    return pl.pallas_call(
+        functools.partial(layer_kernel, n_kv, n_tp),
+        out_shape=jax.ShapeDtypeStruct((batch, col), BF16),
+        in_specs=[pl.BlockSpec(memory_space=pltpu.SMEM)]
+        + [in_vmem] * 7
+        + [pl.BlockSpec(memory_space=pl.ANY)] * len(weights),
+        out_specs=in_vmem,
+        scratch_shapes=scratch,
+        compiler_params=pltpu.CompilerParams(
+            collective_id=0, has_side_effects=True, vmem_limit_bytes=58 * 1024 * 1024
+        ),
+    )(
+        lengths,
+        tokens,
+        gain_attn[None, :],
+        gain_latent[None, :],
+        gain_mlp[None, :],
+        coarse,
+        fine,
+        freq_row,
+        *weights,
+    )
+
+
 def solution(mesh):
+    n_kv, n_tp = mesh.shape["kv"], mesh.shape["tp"]
+
+    def step(*args):
+        batch = args[0].shape[0]
+        seqs = args[-1].shape[0]
+        group = seqs * (args[8].shape[1] // NOPE)
+        if group % 8 == 0 and group * n_tp <= 128 and batch % 16 == 0:
+            return fused(n_kv, n_tp, *args)
+        return per_device(*args)
+
     in_specs = (
         P(None, ("kv", "tp")),
         P(),
@@ -199,5 +718,5 @@
     )
     out_specs = P(None, ("kv", "tp"))
     return jax.shard_map(
-        per_device, mesh=mesh, in_specs=in_specs, out_specs=out_specs, check_vma=False
-    )
+        step, mesh=mesh, in_specs=in_specs, out_specs=out_specs, check_vma=False
+    )

time: 233 us -> 56.2 us (0.24)
  waiting for transfers between devices: 103 us -> 0 us
  blocking collectives: 80 us -> 0 us
  Pallas kernels: 0 us -> 51 us
  matrix products: 16.3 us -> 0 us
  between operations: 13.3 us -> 0.01 us
  other arithmetic: 9.51 us -> 0 us
  starting transfers between devices: 7.03 us -> 0 us
  local copies, waits for them, and re-layouts: 2.62 us -> 4.96 us
    psum x1 -> x0, waiting for transfers between devices: 52.4 us -> none  [per_device(): attn_sum = lax.psum(attn_part, 'tp')]
    pallas_call x0 -> x1, Pallas kernels: none -> 51 us  [fused(): pl.pallas_call(functools.partial(layer_kernel, n_kv, n_tp), out_shape=jax...]
    all_gather x5 -> x0, blocking collectives: 45.8 us -> none  [the longest x3 23 us: merged_2(): lax.all_gather(part.astype(kind), axis)]
    reduce_scatter x2 -> x0, waiting for transfers between devices: 43.8 us -> none  [the longest x1 23.3 us: per_device(): lax.psum_scatter(up_part, 'kv', scatter_dimension=1, tiled=True)]
    psum x1 -> x0, blocking collectives: 17 us -> none  [per_device(): lax.psum((square_piece, part_nope, part_rope, part_latent, part_key), 'kv')]
    dot_general x14 -> x0, matrix products: 16.3 us -> none  [the longest x1 3.5 us: per_device(): up_part = jnp.dot(scaled2, w_up, preferred_element_type=jnp.float32)]
    unnamed x1 -> x0, blocking collectives: 8.89 us -> none
    all_to_all x1 -> x0, blocking collectives: 8.3 us -> none  [per_device(): lax.all_to_all(o_latent, 'tp', split_axis=1, concat_axis=0, tiled=True)]
  transfers between devices with their start and end apart: 5 -> 0, of which waited for: 5 -> 0; matrix products, arithmetic and copies ran while one was open for 2% -> 0% of each run, Pallas kernels for 0% -> 0%
where the time goes in v1:
time: 56.2 us; the launch traced here: 56 us
  Pallas kernels  51 us (91%)
  local copies, waits for them, and re-layouts  4.96 us (9%)
    pallas_call x1, Pallas kernels, fused(): pl.pallas_call(functools.partial(layer_kernel, n_kv, n_tp), out_shape=jax...  51 us
    unnamed x3, local copies, waits for them, and re-layouts  4.96 us

profile of v1, /device:TPU:0, one launch (start us, length us, event | category | flops | bytes accessed | tf_op | source)
XLA Modules:
  0.0 56.0 jit_solution(10688084102773545296)
XLA Ops:
  0.0 1.7 %copy.20.h_key = bf16[1024,64]{1,0:T(8,128)(2,1)} copy(bf16[1024,64]{0,1:T(8,128)(2,1)} %param.25) | data formatting | bytes 262144 | tf_op args[6]
  1.7 1.9 %copy.21.h_cr = bf16[2,1024,64]{2,1,0:T(8,128)(2,1)} copy(bf16[2,1024,64]{1,2,0:T(8,128)(2,1)} %param.34) | data formatting | bytes 524288 | tf_op args[15]
  3.7 51.0 %shard_map.181 = bf16[16,128]{1,0:T(8,128)(2,1)} custom-call(s32[16]{0:T(128)} %len_ref.1, bf16[16,128]{1,0:T(8,128)(2,1)} %tok_ref.1, f32[1,1024]{1,0:T(1,128)} %bitcast.3, f32[1,512]{1,0:T(1,128)} %bitcast.5, f32[1,1024]{1,0:T(1,128)} %bitcast.4, f32[2,128,64]{2,1,0:T(8,128)} %constant.6.clone.coarse_ref, f32[2,32,64]{2,1,0:T(8,128)} %constant.7.clone.fine_ref, ...), custom_call_target="tpu_custom_call" | custom-call | tf_op jit(solution)/shard_map/pallas_call | solution.py:666
  54.7 1.3 %copy.23 = bf16[16,128]{1,0:T(8,128)(2,1)} copy(bf16[16,128]{1,0:T(8,128)(2,1)} %shard_map.181) | data formatting | bytes 8192

commit v2 on v1

--- a/solution.py
+++ b/solution.py
@@ -186,7 +186,6 @@
 MESH = pl.DeviceIdType.MESH
 BF16 = jnp.bfloat16
 F32 = jnp.float32
-FINE = 32
 
 
 def dot(a, b):
@@ -209,9 +208,8 @@
     gain_attn,
     gain_latent,
     gain_mlp,
-    coarse_ref,
-    fine_ref,
     freq_ref,
+    h_turn,
     h_qn,
     h_qr,
     h_lat,
@@ -235,6 +233,7 @@
     w_down,
     c_lat,
     c_rope,
+    turn,
     rot,
     tok_all,
     qp_own,
@@ -259,8 +258,6 @@
     up_in,
     sq2_own,
     sq2_in,
-    act_own,
-    act_all,
     dn_own,
     dn_in,
     load_sem,
@@ -285,6 +282,7 @@
         ("qr", h_qr, w_qr),
         ("lat", h_lat, w_lat),
         ("key", h_key, w_key),
+        ("turn", h_turn.at[kv], turn),
         ("cr", h_cr, c_rope),
         ("kup", h_kup, w_kup),
         ("cl", h_cl, c_lat),
@@ -310,13 +308,16 @@
     started = []
 
     def send(axis, d, source, target):
+        return send_to({axis: peer(axis, d)}, source, target)
+
+    def send_to(device, source, target):
         i = len(started)
         copy = pltpu.make_async_remote_copy(
             src_ref=source,
             dst_ref=target,
             send_sem=send_sem.at[i],
             recv_sem=recv_sem.at[i],
-            device_id={axis: lax.rem(here[axis] + d, size[axis])},
+            device_id=device,
             device_id_type=MESH,
         )
         copy.start()
@@ -357,27 +358,15 @@
     tok_copies = [send("tp", d, tok_ref, tok_all.at[tp]) for d in range(1, n_tp)]
     tok_all[tp] = tok_ref[...]
 
+    loads["turn"].wait()
     loads["cr"].wait()
     half = ROPE // 2
-    s_row = iota((ROPE, ROPE), 0)
-    s_col = iota((ROPE, ROPE), 1)
-    swap = jnp.where(s_row == s_col + half, -1.0, 0.0) + jnp.where(s_row + half == s_col, 1.0, 0.0)
-    swap = swap.astype(BF16)
-    n_coarse = cache_dev // FINE
-    first = pl.multiple_of(kv * n_coarse, 8)
-    cos_a = coarse_ref[0, pl.ds(first, n_coarse), :]
-    sin_a = coarse_ref[1, pl.ds(first, n_coarse), :]
-    cos_b = fine_ref[0]
-    sin_b = fine_ref[1]
-    for i in range(n_coarse):
-        part = pl.ds(i * FINE, FINE)
-        ca, sa = cos_a[i : i + 1], sin_a[i : i + 1]
-        cos_p = ca * cos_b - sa * sin_b
-        sin_p = sa * cos_b + ca * sin_b
-        for s in range(seqs):
-            keys = c_rope[s, part, :]
-            turned = keys.astype(F32) * cos_p + dot(keys, swap) * sin_p
-            rot[s, part, :] = turned.astype(BF16)
+    key_cos, key_sin = turn[0], turn[1]
+    for s in range(seqs):
+        lower = c_rope[s, :half].astype(F32)
+        upper = c_rope[s, half:].astype(F32)
+        rot[s, :half] = (lower * key_cos - upper * key_sin).astype(BF16)
+        rot[s, half:] = (upper * key_cos + lower * key_sin).astype(BF16)
 
     arrive(tok_copies)
     toks = jnp.concatenate([tok_all[i] for i in range(n_tp)], axis=1)
@@ -395,7 +384,7 @@
     loads["lat"].wait()
     lat_own[:, :rank] = dot(own_scaled, w_lat[...])
     loads["key"].wait()
-    lat_own[:, rank : rank + ROPE] = dot(own_scaled, w_key[...])
+    lat_own[:, rank : rank + ROPE] = dot_nt(own_scaled, w_key[...])
     lat_own[:, rank + ROPE :] = jnp.broadcast_to(
         jnp.sum(own_tok * own_tok, axis=1, keepdims=True), (group, ROPE)
     )
@@ -462,7 +451,7 @@
     rope_query = q_low[:, rank : rank + ROPE]
     scores = None
     for s in range(seqs):
-        one = dot_nt(latent_query, c_lat[s]) + dot_nt(rope_query, rot[s])
+        one = dot_nt(latent_query, c_lat[s]) + dot(rope_query, rot[s])
         scores = one if scores is None else jnp.where(row_seq == s, one, scores)
     scores = scores * score_scale
     live = kv * cache_dev + iota((rows, cache_dev), 1) < own_len
@@ -478,36 +467,58 @@
     diag = iota((rows, 128), 0) == iota((rows, 128), 1)
     max_row = jnp.sum(jnp.where(diag, block_max, 0.0), axis=0, keepdims=True)
     sum_row = jnp.sum(jnp.where(diag, block_sum, 0.0), axis=0, keepdims=True)
+    half_z, core = tp // 2, lax.rem(tp, 2)
+    n_z, part_rows = n_tp // 2, 2 * group
+    parts = list(range(n_z // 2, n_z)) + list(range(1, n_z // 2)) + [0]
+    parts = list(dict.fromkeys(parts))
     st_own[...] = jnp.where(iota((8, 128), 0) == 0, max_row, sum_row)
-    bo_copies = [send("kv", d, bo_own, bo_in.at[d - 1]) for d in range(1, n_kv)]
     st_copies = [send("kv", d, st_own, st_in.at[d - 1]) for d in range(1, n_kv)]
+    part_of, bo_copies = {}, {}
+    for dz in parts:
+        part_of[dz] = lax.rem(half_z + dz, n_z)
+        span = pl.ds(pl.multiple_of(part_of[dz] * part_rows, 16), part_rows)
+        bo_copies[dz] = [
+            send("kv", d, bo_own.at[span], bo_in.at[d - 1, span]) for d in range(1, n_kv)
+        ]
 
     self_score = (
         jnp.sum(q_all[:, :rank] * latent_rows, axis=1, keepdims=True)
         + jnp.sum(q_all[:, rank:] * key_rows, axis=1, keepdims=True)
     ) * score_scale
+    self_row = jnp.sum(jnp.where(diag, self_score, 0.0), axis=0, keepdims=True)
     arrive(st_copies)
-    maxes, sums = [block_max], [block_sum]
-    for d in range(n_kv - 1):
-        maxes.append(jnp.sum(jnp.where(diag, st_in[d, 0:1, :], 0.0), axis=1, keepdims=True))
-        sums.append(jnp.sum(jnp.where(diag, st_in[d, 1:2, :], 0.0), axis=1, keepdims=True))
-    top = self_score
-    for one in maxes:
+    max_rows = [max_row] + [st_in[d, 0:1, :] for d in range(n_kv - 1)]
+    sum_rows = [sum_row] + [st_in[d, 1:2, :] for d in range(n_kv - 1)]
+    top = self_row
+    for one in max_rows:
         top = jnp.maximum(top, one)
-    weights = [total * jnp.exp(one - top) for one, total in zip(maxes, sums)]
-    self_weight = jnp.exp(self_score - top)
-    whole = self_weight
-    for one in weights:
-        whole = whole + one
-    blend = self_weight * latent_rows + weights[0] * bo_own[...].astype(F32)
-    for d in range(n_kv - 1):
-        bo_copies[d].wait_recv()
-        blend = blend + weights[d + 1] * bo_in[d].astype(F32)
-    o_own[...] = (blend / whole).reshape(n_tp, group, rank).astype(BF16)
-    o_copies = [
-        send("tp", d, o_own.at[peer("tp", d)], o_in.at[tp]) for d in range(1, n_tp)
-    ]
-    o_in[tp] = o_own[tp]
+    weight_rows = [total * jnp.exp(one - top) for one, total in zip(max_rows, sum_rows)]
+    weight_rows.append(jnp.exp(self_row - top))
+    whole_row = weight_rows[0]
+    for one in weight_rows[1:]:
+        whole_row = whole_row + one
+    o_copies = []
+    for dz in parts:
+        at = part_of[dz]
+        span = pl.ds(pl.multiple_of(at * part_rows, 16), part_rows)
+        mine = iota((part_rows, 128), 0) + at * part_rows == iota((part_rows, 128), 1)
+
+        def column(row):
+            return jnp.sum(jnp.where(mine, row, 0.0), axis=1, keepdims=True)
+
+        arrive(bo_copies[dz])
+        blend = column(weight_rows[-1]) * latent_rows[:part_rows]
+        blend = blend + column(weight_rows[0]) * bo_own[span, :].astype(F32)
+        for d in range(n_kv - 1):
+            blend = blend + column(weight_rows[d + 1]) * bo_in[d, span, :].astype(F32)
+        blend = (blend / column(whole_row)).reshape(2, group, rank)
+        o_own[pl.ds(2 * at, 2)] = blend.astype(BF16)
+        for dc in range(2):
+            target = 2 * at + lax.rem(core + dc, 2)
+            if dz == 0 and dc == 0:
+                o_in[tp] = o_own[tp]
+            else:
+                o_copies.append(send_to({"tp": target}, o_own.at[target], o_in.at[tp]))
     loads["vup"].wait()
     loads["out"].wait()
     arrive(o_copies)
@@ -538,24 +549,18 @@
     sq2_copies = [send("kv", d, sq2_own, sq2_in.at[d - 1]) for d in range(1, n_kv)]
     share = w_up.shape[1] // n_kv
     up_copies = []
-    for d in range(1, n_kv):
-        cols = pl.ds(pl.multiple_of(peer("kv", d) * share, 128), share)
-        up_own[d - 1] = dot(scaled2, w_up[:, cols]).astype(BF16)
-        up_copies.append(send("kv", d, up_own.at[d - 1], up_in.at[d - 1]))
-    up_sum = dot(scaled2, w_up[:, pl.ds(pl.multiple_of(kv * share, 128), share)])
-    for d in range(n_kv - 1):
-        up_copies[d].wait_recv()
-        up_sum = up_sum + up_in[d].astype(F32)
-    act_own[...] = jnp.square(jnp.maximum(up_sum, 0.0)).astype(BF16)
-    act_copies = [send("kv", d, act_own, act_all.at[d - 1]) for d in range(1, n_kv)]
+    for i in range(n_kv):
+        up_own[i] = dot(scaled2, w_up[:, i * share : (i + 1) * share]).astype(BF16)
+        up_copies.append([send("kv", d, up_own.at[i], up_in.at[d - 1, i]) for d in range(1, n_kv)])
     loads["down"].wait()
-    down = dot(act_own[...], w_down[pl.ds(pl.multiple_of(kv * share, 128), share), :])
-    for d in range(1, n_kv):
-        act_copies[d - 1].wait_recv()
-        source = lax.rem(kv + n_kv - d, n_kv)
-        down = down + dot(
-            act_all[d - 1], w_down[pl.ds(pl.multiple_of(source * share, 128), share), :]
-        )
+    down = jnp.zeros((batch, w_down.shape[1]), F32)
+    for i in range(n_kv):
+        arrive(up_copies[i])
+        up_sum = up_own[i].astype(F32)
+        for d in range(n_kv - 1):
+            up_sum = up_sum + up_in[d, i].astype(F32)
+        active = jnp.square(jnp.maximum(up_sum, 0.0)).astype(BF16)
+        down = down + dot(active, w_down[i * share : (i + 1) * share, :])
     for i in range(n_tp):
         dn_own[i] = down[:, i * col : (i + 1) * col].astype(BF16)
     dn_copies = [
@@ -602,18 +607,17 @@
     share = w_up.shape[1] // n_kv
     half = ROPE // 2
     freq = np.float32(10000.0) ** (-np.arange(half, dtype=np.float32) / np.float32(half))
-    freq = freq.astype(np.float64)
-    lanes = np.tile(freq, 2)[None, :]
-    coarse = np.arange(n_kv * cache_dev // FINE)[:, None] * FINE * lanes
-    fine = np.arange(FINE)[:, None] * lanes
-    coarse = jnp.asarray(np.stack([np.cos(coarse), np.sin(coarse)]), F32)
-    fine = jnp.asarray(np.stack([np.cos(fine), np.sin(fine)]), F32)
+    angles = freq.astype(np.float64)[:, None] * np.arange(n_kv * cache_dev)
+    turns = np.stack([np.cos(angles), np.sin(angles)]).reshape(2, half, n_kv, cache_dev)
+    turns = jnp.asarray(turns.transpose(2, 0, 1, 3), F32)
     wide_lanes = max(heads * ROPE, 128)
     freq_row = jnp.asarray(np.tile(np.tile(freq, wide_lanes // half)[None, :], (8, 1)), F32)
 
     def vm(*shape, kind=BF16):
         return pltpu.VMEM(shape, kind)
 
+    w_rope_key = w_rope_key.T
+    cache_rope = jnp.swapaxes(cache_rope, 1, 2)
     weights = (
         w_query_nope,
         w_query_rope,
@@ -630,6 +634,7 @@
     k, t = n_kv - 1, n_tp - 1
     qp = heads * (NOPE + ROPE)
     scratch = [vm(*w.shape, kind=w.dtype) for w in weights] + [
+        vm(2, half, cache_dev, kind=F32),
         vm(*cache_rope.shape),
         vm(n_tp, batch, col),
         vm(batch, qp),
@@ -650,25 +655,23 @@
         vm(t, batch, col),
         vm(batch, col),
         vm(n_tp, batch, col),
-        vm(k, batch, share),
-        vm(k, batch, share),
+        vm(n_kv, batch, share),
+        vm(k, n_kv, batch, share),
         vm(batch, 128, kind=F32),
         vm(k, batch, 128, kind=F32),
-        vm(batch, share),
-        vm(k, batch, share),
         vm(n_tp, batch, col),
         vm(t, batch, col),
-        pltpu.SemaphoreType.DMA((len(weights),)),
-        pltpu.SemaphoreType.DMA((6 * t + 8 * k,)),
-        pltpu.SemaphoreType.DMA((6 * t + 8 * k,)),
+        pltpu.SemaphoreType.DMA((len(weights) + 1,)),
+        pltpu.SemaphoreType.DMA((6 * t + (5 + n_kv + n_tp // 2) * k,)),
+        pltpu.SemaphoreType.DMA((6 * t + (5 + n_kv + n_tp // 2) * k,)),
     ]
     in_vmem = pl.BlockSpec(memory_space=pltpu.VMEM)
     return pl.pallas_call(
         functools.partial(layer_kernel, n_kv, n_tp),
         out_shape=jax.ShapeDtypeStruct((batch, col), BF16),
         in_specs=[pl.BlockSpec(memory_space=pltpu.SMEM)]
-        + [in_vmem] * 7
-        + [pl.BlockSpec(memory_space=pl.ANY)] * len(weights),
+        + [in_vmem] * 5
+        + [pl.BlockSpec(memory_space=pl.ANY)] * (1 + len(weights)),
         out_specs=in_vmem,
         scratch_shapes=scratch,
         compiler_params=pltpu.CompilerParams(
@@ -680,9 +683,8 @@
         gain_attn[None, :],
         gain_latent[None, :],
         gain_mlp[None, :],
-        coarse,
-        fine,
         freq_row,
+        turns,
         *weights,
     )
 
@@ -694,7 +696,7 @@
         batch = args[0].shape[0]
         seqs = args[-1].shape[0]
         group = seqs * (args[8].shape[1] // NOPE)
-        if group % 8 == 0 and group * n_tp <= 128 and batch % 16 == 0:
+        if group % 8 == 0 and group * n_tp <= 128 and batch % 16 == 0 and n_tp % 2 == 0:
             return fused(n_kv, n_tp, *args)
         return per_device(*args)
 

time: 56.2 us -> 49.9 us (0.89)
  local copies, waits for them, and re-layouts: 4.96 us -> 1.28 us
  Pallas kernels: 51 us -> 48.4 us
    unnamed x3 -> x1, local copies, waits for them, and re-layouts: 4.96 us -> 1.28 us
    pallas_call x1, Pallas kernels: 51 us -> 48.4 us  [fused(): pl.pallas_call(functools.partial(layer_kernel, n_kv, n_tp), out_shape=jax...]
where the time goes in v2:
time: 49.9 us; the launch traced here: 49.7 us
  Pallas kernels  48.4 us (97%)
  local copies, waits for them, and re-layouts  1.28 us (3%)
    pallas_call x1, Pallas kernels, fused(): pl.pallas_call(functools.partial(layer_kernel, n_kv, n_tp), out_shape=jax...  48.4 us
    unnamed x1, local copies, waits for them, and re-layouts  1.28 us

profile of v2, /device:TPU:0, one launch (start us, length us, event | category | flops | bytes accessed | tf_op | source)
XLA Modules:
  0.0 49.7 jit_solution(304520009760731909)
XLA Ops:
  0.0 48.4 %shard_map.172 = bf16[16,128]{1,0:T(8,128)(2,1)} custom-call(s32[16]{0:T(128)} %len_ref.1, bf16[16,128]{1,0:T(8,128)(2,1)} %tok_ref.1, f32[1,1024]{1,0:T(1,128)} %bitcast.7, f32[1,512]{1,0:T(1,128)} %bitcast.9, f32[1,1024]{1,0:T(1,128)} %bitcast.8, f32[8,256]{1,0:T(8,128)} %constant.5.clone.freq_ref, f32[4,2,32,1024]{3,2,1,0:T(8,128)} %constant.4.clone.h_turn, ...), custom_call_target="tpu_custom_call" | custom-call | tf_op jit(solution)/shard_map/pallas_call | solution.py:669
  48.4 1.3 %copy.20 = bf16[16,128]{1,0:T(8,128)(2,1)} copy(bf16[16,128]{1,0:T(8,128)(2,1)} %shard_map.172) | data formatting | bytes 8192
